TPU v7x, 32 devices: a whole 2x2x4 slice. The times are simulated.
32 devices in a mesh: ra: 8 (over z, y), cb: 4 (over x, core).
Axes of the slice: x: 2, y: 2, z: 4, core: 2. Of those that a mesh axis runs over, the one named last changes fastest.
Arguments:
- tokens: bfloat16 [512, 4096], P(None, 'cb'), may hold values from -82 to 82
- gate_weight: float32 [2, 4096, 11264], P(None, 'cb', 'ra'), may hold values from -0.09375 to 0.09375
- up_weight: float32 [2, 4096, 11264], P(None, 'cb', 'ra'), may hold values from -0.09375 to 0.09375
- down_weight: float32 [2, 11264, 4096], P(None, 'ra', 'cb'), may hold values from -0.0546875 to 0.0546875
- gate_scale: float32 [2, 11264], P(None, 'ra'), may hold values from 0.5 to 2
- up_scale: float32 [2, 11264], P(None, 'ra'), may hold values from 0.5 to 2
- down_scale: float32 [2, 4096], P(None, 'cb'), may hold values from 0.5 to 2
- norm_gain: float32 [2, 4096], P(None, 'cb'), may hold values from 0.1 to 1.9
- conv_taps: float32 [2, 3, 11264], P(None, None, 'ra'), may hold values from -3 to 3
- conv_bias: float32 [2, 11264], P(None, 'ra'), may hold values from -3 to 3
Outputs:
- layer_out: bfloat16 [512, 4096], P(None, 'cb')
All inputs are finite; a program needn't handle non-finite values.
Results may differ from a plain program's by a relative error of at most 0.012.
Values may be sent and summed in bfloat16 or wider, within the bound.
A program may use at most 128 MiB of HBM per device.

v0:
```python
import jax
import jax.numpy as jnp
from jax import lax
from jax.sharding import PartitionSpec as P

D = 4096
LAYERS = 2
norm_eps = 1e-06
residual_scale = 0.25


def activate(gate, upward, taps, bias):
    padded = jnp.pad(gate, ((1, 1), (0, 0)))
    mixed = taps[0] * padded[:-2] + taps[1] * padded[1:-1] + taps[2] * padded[2:] + bias
    return (jax.nn.silu(mixed) * upward).astype(jnp.bfloat16)


def per_device(
    tokens,
    gate_weight,
    up_weight,
    down_weight,
    gate_scale,
    up_scale,
    down_scale,
    norm_gain,
    conv_taps,
    conv_bias,
):
    hstate = tokens
    for layer in range(LAYERS):
        wide = hstate.astype(jnp.float32)
        squares_part = jnp.sum(wide * wide, axis=1)
        operand = (wide * norm_gain[layer]).astype(jnp.bfloat16)
        gate_part = jnp.dot(
            operand, gate_weight[layer].astype(jnp.bfloat16), preferred_element_type=jnp.float32
        )
        up_part = jnp.dot(
            operand, up_weight[layer].astype(jnp.bfloat16), preferred_element_type=jnp.float32
        )
        gate_sum, up_sum, square_sum = lax.psum((gate_part, up_part, squares_part), "cb")
        rscale = lax.rsqrt(square_sum / D + norm_eps)[:, None]
        gate = gate_sum * rscale * gate_scale[layer]
        upward = up_sum * rscale * up_scale[layer]
        hidden = activate(gate, upward, conv_taps[layer], conv_bias[layer])
        term = jnp.dot(
            hidden, down_weight[layer].astype(jnp.bfloat16), preferred_element_type=jnp.float32
        )
        branch = lax.psum(term, "ra") * down_scale[layer]
        hstate = (residual_scale * wide + branch).astype(jnp.bfloat16)
    return hstate


def solution(mesh):
    in_specs = (
        P(None, "cb"),
        P(None, "cb", "ra"),
        P(None, "cb", "ra"),
        P(None, "ra", "cb"),
        P(None, "ra"),
        P(None, "ra"),
        P(None, "cb"),
        P(None, "cb"),
        P(None, None, "ra"),
        P(None, "ra"),
    )
    out_specs = P(None, "cb")
    return jax.shard_map(
        per_device, mesh=mesh, in_specs=in_specs, out_specs=out_specs, check_vma=False
    )
```

profile of v0, /device:TPU:0, one launch (start us, length us, event | category | flops | bytes accessed | tf_op | source)
XLA Modules:
  0.0 497.1 jit_solution(6274130120586286872)
XLA Ops:
  6.5 0.8 fusion.24
  7.3 4.9 convert.13
  12.2 9.4 %convert.12 = bf16[2,1024,1408]{2,1,0:T(8,128)(2,1)} convert(f32[2,1024,1408]{2,1,0:T(8,128)} %param.11) | non-fusion elementwise | flops 2883584 | bytes 17301504 | tf_op jit(solution)/shard_map/convert.5
  21.6 3.4 fusion.4
  25.1 3.4 fusion.5
  28.5 7.7 %convert.14 = bf16[2,1408,1024]{2,1,0:T(8,128)(2,1)} convert(f32[2,1408,1024]{2,1,0:T(8,128)} %param.13) | non-fusion elementwise | flops 2883584 | bytes 17301504 | tf_op jit(solution)/shard_map/convert.3
  36.2 0.3 fusion.9
  36.5 9.1 %psum.57 = f32[512]{0:T(512)S(1)} all-reduce(f32[512]{0:T(512)S(1)} %fusion.9), channel_id=1, replica_groups=mesh['ra'=8,'cb'=4] {'cb'}, use_global_device_ids=true, to_apply=%region_2.0 | all-reduce | flops 512 | bytes 4096 | tf_op jit(solution)/shard_map/psum | solution.py:41
  45.7 0.1 slice_reduce_fusion.5
  45.8 96.7 %all-reduce.15.cloned.1.call-done = (f32[512,1408]{1,0:T(8,128)}, f32[512,1408]{1,0:T(8,128)}) async-done(((f32[512,1408]{1,0:T(8,128)}, f32[512,1408]{1,0:T(8,128)}), (f32[512,1408]{1,0:T(8,128)}, f32[512,1408]{1,0:T(8,128)})) %all-reduce.15.cloned.1.call-update) | async-done | bytes 5767184 | tf_op jit(solution)/shard_map/psum | solution.py:41
  142.5 2.3 multiply_multiply_fusion.1
  144.8 1.2 copy-done
  146.0 6.1 %fusion.3 = f32[512,1024]{1,0:T(8,128)} fusion(bf16[2,1408,1024]{2,1,0:T(8,128)(2,1)S(1)} %copy-done, f32[512,1408]{1,0:T(8,128)} %get-tuple-element.19, f32[512,1408]{1,0:T(8,128)S(1)} %multiply_multiply_fusion.1, f32[1408]{0:T(1024)S(1)} %get-tuple-element.14, f32[1408]{0:T(1024)S(1)} %get-tuple-element.27, f32[1408]{0:T(1024)S(1)} %get-tuple-element.6, ...), kind=kOutput, calls=%fused_computation.13 | convolution fusion | flops 1486487552 | bytes 10790912 | tf_op jit(solution)/shard_map/dot_general | solution.py:46
  152.2 102.5 %all-reduce.9.cloned.1.call-done = f32[512,1024]{1,0:T(8,128)} async-done(((f32[512,1024]{1,0:T(8,128)}), f32[512,1024]{1,0:T(8,128)}) %all-reduce.9.cloned.1.call-update) | async-done | bytes 2097168 | tf_op jit(solution)/shard_map/psum | solution.py:49
  254.7 2.3 fusion.13
  257.0 5.3 %fusion.2 = f32[512,1408]{1,0:T(8,128)} fusion(bf16[2,1024,1408]{2,1,0:T(8,128)(2,1)} %convert.12, bf16[512,1024]{1,0:T(8,128)(2,1)S(1)} %get-tuple-element.22, f32[1024]{0:T(1024)S(1)} %bitcast.26), kind=kOutput, calls=%fused_computation.11 | convolution fusion | flops 1477967872 | bytes 6819840 | tf_op jit(solution)/shard_map/dot_general | solution.py:35
  262.3 3.5 fusion.1
  265.8 6.3 %psum.61 = f32[512]{0:T(512)S(1)} all-reduce(f32[512]{0:T(512)S(1)} %get-tuple-element.21), channel_id=1, replica_groups=mesh['ra'=8,'cb'=4] {'cb'}, use_global_device_ids=true, to_apply=%region_7.8 | all-reduce | flops 512 | bytes 4096 | tf_op jit(solution)/shard_map/psum | solution.py:41
  272.2 104.1 %all-reduce.13.cloned.1.call-done = (f32[512,1408]{1,0:T(8,128)}, f32[512,1408]{1,0:T(8,128)}) async-done(((f32[512,1408]{1,0:T(8,128)}, f32[512,1408]{1,0:T(8,128)}), (f32[512,1408]{1,0:T(8,128)}, f32[512,1408]{1,0:T(8,128)})) %all-reduce.13.cloned.1.call-update) | async-done | bytes 5767184 | tf_op jit(solution)/shard_map/psum | solution.py:41
  376.3 2.3 multiply_multiply_fusion
  378.6 0.4 copy-done.9
  379.0 6.0 %fusion = f32[512,1024]{1,0:T(8,128)} fusion(bf16[2,1408,1024]{2,1,0:T(8,128)(2,1)} %convert.14, f32[512,1408]{1,0:T(8,128)S(1)} %copy-done.9, f32[512,1408]{1,0:T(8,128)S(1)} %multiply_multiply_fusion, f32[1408]{0:T(1024)S(1)} %get-tuple-element.13, f32[1408]{0:T(1024)S(1)} %get-tuple-element.28, f32[1408]{0:T(1024)S(1)} %get-tuple-element.9, ...), kind=kOutput, calls=%fused_computation.7 | convolution fusion | flops 1486487552 | bytes 10778112 | tf_op jit(solution)/shard_map/dot_general | solution.py:46
  385.0 102.6 %all-reduce.11.cloned.1.call-done = f32[512,1024]{1,0:T(8,128)} async-done(((f32[512,1024]{1,0:T(8,128)}), f32[512,1024]{1,0:T(8,128)}) %all-reduce.11.cloned.1.call-update) | async-done | bytes 2097168 | tf_op jit(solution)/shard_map/psum | solution.py:49
  487.6 2.9 fusion.11
  (36 shorter events, 0.4 us)
Async XLA Ops:
  6.5 136.0 %all-reduce.15.cloned.1.call-start = ((), (), s32[]{:S(2)}) async-start(), calls=%async_computation.3 | async-start | bytes 11534336 | tf_op jit(solution)/shard_map/psum | solution.py:41
  12.2 9.4 %copy-start.1 = (bf16[2,1024,1408]{2,1,0:T(8,128)(2,1)}, bf16[2,1024,1408]{2,1,0:T(8,128)(2,1)S(1)}, u32[]{:S(2)}) copy-start(bf16[2,1024,1408]{2,1,0:T(8,128)(2,1)S(1)} %convert.13) | copy-start | bytes 17301508
  12.2 9.4 %copy-start.3 = (bf16[512,1024]{1,0:T(8,128)(2,1)S(1)}, bf16[512,1024]{1,0:T(8,128)(2,1)}, u32[]{:S(2)}) copy-start(bf16[512,1024]{1,0:T(8,128)(2,1)} %param.10) | copy-start | bytes 3145732
  21.6 3.4 copy-start.2
  28.4 17.2 %copy-start.5 = (f32[2,1408]{1,0:T(2,128)S(1)}, f32[2,1408]{1,0:T(2,128)}, u32[]{:S(2)}) copy-start(f32[2,1408]{1,0:T(2,128)} %param.14) | copy-start | bytes 33796
  28.4 17.2 %copy-start.6 = (f32[2,1408]{1,0:T(2,128)S(1)}, f32[2,1408]{1,0:T(2,128)}, u32[]{:S(2)}) copy-start(f32[2,1408]{1,0:T(2,128)} %param.15) | copy-start | bytes 33796
  28.5 17.2 %copy-start.7 = (f32[2,1408]{1,0:T(2,128)S(1)}, f32[2,1408]{1,0:T(2,128)}, u32[]{:S(2)}) copy-start(f32[2,1408]{1,0:T(2,128)} %param.19) | copy-start | bytes 33796
  28.5 17.3 %copy-start.4 = (f32[2,3,1408]{2,0,1:T(2,128)S(1)}, f32[2,3,1408]{2,0,1:T(2,128)}, u32[]{:S(2)}) copy-start(f32[2,3,1408]{2,0,1:T(2,128)} %param.18) | copy-start | bytes 101380
  28.5 226.3 %all-reduce.9.cloned.1.call-start = ((), (), s32[]{:S(2)}) async-start(), calls=%async_computation | async-start | bytes 4194304 | tf_op jit(solution)/shard_map/psum | solution.py:49
  142.5 3.5 copy-start
  146.0 6.1 %copy-start.8 = (f32[2,1024]{1,0:T(2,128)S(1)}, f32[2,1024]{1,0:T(2,128)}, u32[]{:S(2)}) copy-start(f32[2,1024]{1,0:T(2,128)} %param.16) | copy-start | bytes 24580
  152.1 224.2 %all-reduce.13.cloned.1.call-start = ((), (), s32[]{:S(2)}) async-start(), calls=%async_computation.2 | async-start | bytes 11534336 | tf_op jit(solution)/shard_map/psum | solution.py:41
  254.7 7.6 %slice-start = ((s8[5767168]{0:T(1024)(128)(4,1)}), s8[4194304]{0:T(1024)(128)(4,1)S(1)}, s32[]{:S(2)}) async-start(s8[5767168]{0:T(1024)(128)(4,1)} %bitcast.22), calls=%async_computation.4 | async-start | bytes 8388608
  257.0 5.3 %slice-start.1 = ((s8[5767168]{0:T(1024)(128)(4,1)}), s8[1572864]{0:T(1024)(128)(4,1)S(1)}, s32[]{:S(2)}) async-start(s8[5767168]{0:T(1024)(128)(4,1)} %bitcast.22), calls=%async_computation.5 | async-start | bytes 3145728
  265.8 221.8 %all-reduce.11.cloned.1.call-start = ((), (), s32[]{:S(2)}) async-start(), calls=%async_computation.1 | async-start | bytes 4194304 | tf_op jit(solution)/shard_map/psum | solution.py:49
  376.3 2.7 copy-start.9
Sparse Core Ops, SparseCore 0:
  28.6 113.9 all-reduce.14
  152.2 102.4 all-reduce.8
  265.9 110.3 all-reduce.12
  385.1 102.4 all-reduce.10
where the time goes:
time: 497 us
  waiting for transfers between devices  406 us (82%)
  other arithmetic  31.9 us (6%)
  matrix products  27.6 us (6%)
  blocking collectives  15.4 us (3%)
  between operations  13.3 us (3%)
    psum x2, waiting for transfers between devices, per_device(): branch = lax.psum(term, 'ra') * down_scale[layer]  205 us
    psum x2, waiting for transfers between devices, per_device(): lax.psum((gate_part, up_part, squares_part), 'cb')  201 us
    another operation x3, other arithmetic  21.9 us
    psum x2, blocking collectives, per_device(): lax.psum((gate_part, up_part, squares_part), 'cb')  15.4 us
    dot_general x2, matrix products, per_device(): jnp.dot(hidden, down_weight[layer].astype(jnp.bfloat16), preferred_elemen...  12 us
  transfers between devices with their start and end apart: 4, of which 4 were waited for; matrix products, arithmetic and copies ran while one was open for 2% of the time, Pallas kernels for 0%

commit v1 on v0

--- a/solution.py
+++ b/solution.py
@@ -7,6 +7,11 @@
 LAYERS = 2
 norm_eps = 1e-06
 residual_scale = 0.25
+
+
+def gather_and_add(array, mesh_axis):
+    parts = lax.all_gather(array, mesh_axis)
+    return jnp.sum(parts, axis=0)
 
 
 def activate(gate, upward, taps, bias):
@@ -46,7 +51,7 @@
         term = jnp.dot(
             hidden, down_weight[layer].astype(jnp.bfloat16), preferred_element_type=jnp.float32
         )
-        branch = lax.psum(term, "ra") * down_scale[layer]
+        branch = gather_and_add(term, "ra") * down_scale[layer]
         hstate = (residual_scale * wide + branch).astype(jnp.bfloat16)
     return hstate
 

time: 497 us -> 760 us (1.53)
  waiting for transfers between devices: 406 us -> 655 us
  other arithmetic: 31.9 us -> 45.9 us
    all_gather x0 -> x2, waiting for transfers between devices: none -> 455 us  [gather_and_add(): parts = lax.all_gather(array, mesh_axis)]
    psum x2 -> x0, waiting for transfers between devices: 205 us -> none  [per_device(): branch = lax.psum(term, 'ra') * down_scale[layer]]
    reduce_sum x0 -> x2, other arithmetic: none -> 15.9 us  [gather_and_add(): return jnp.sum(parts, axis=0)]
  transfers between devices with their start and end apart: 4 -> 4, of which waited for: 4 -> 4; matrix products, arithmetic and copies ran while one was open for 2% -> 1% of each run, Pallas kernels for 0% -> 0%
where the time goes in v1:
time: 760 us
  waiting for transfers between devices  655 us (86%)
  other arithmetic  45.9 us (6%)
  matrix products  27.6 us (4%)
  blocking collectives  15 us (2%)
  between operations  13.3 us (2%)
    all_gather x2, waiting for transfers between devices, gather_and_add(): parts = lax.all_gather(array, mesh_axis)  455 us
    psum x2, waiting for transfers between devices, per_device(): lax.psum((gate_part, up_part, squares_part), 'cb')  200 us
    another operation x3, other arithmetic  21.9 us
    reduce_sum x2, other arithmetic, gather_and_add(): return jnp.sum(parts, axis=0)  15.9 us
  transfers between devices with their start and end apart: 4, of which 4 were waited for; matrix products, arithmetic and copies ran while one was open for 1% of the time, Pallas kernels for 0%

profile of v1, /device:TPU:0, one launch (start us, length us, event | category | flops | bytes accessed | tf_op | source)
XLA Modules:
  0.0 760.0 jit_solution(11928785026625512524)
XLA Ops:
  6.5 0.8 fusion.24
  7.3 4.9 convert.13
  12.2 9.4 %convert.12 = bf16[2,1024,1408]{2,1,0:T(8,128)(2,1)} convert(f32[2,1024,1408]{2,1,0:T(8,128)} %param.11) | non-fusion elementwise | flops 2883584 | bytes 17301504 | tf_op jit(solution)/shard_map/convert.5
  21.6 3.4 fusion.4
  25.0 3.5 fusion.5
  28.6 7.7 %convert.14 = bf16[2,1408,1024]{2,1,0:T(8,128)(2,1)} convert(f32[2,1408,1024]{2,1,0:T(8,128)} %param.13) | non-fusion elementwise | flops 2883584 | bytes 17301504 | tf_op jit(solution)/shard_map/convert.3
  36.5 9.1 %psum.43 = f32[512]{0:T(512)S(1)} all-reduce(f32[512]{0:T(512)S(1)} %fusion.9), channel_id=1, replica_groups=mesh['ra'=8,'cb'=4] {'cb'}, use_global_device_ids=true, to_apply=%region_2.0 | all-reduce | flops 512 | bytes 4096 | tf_op jit(solution)/shard_map/psum | solution.py:46
  45.9 96.7 %all-reduce.9.cloned.1.call-done = (f32[512,1408]{1,0:T(8,128)}, f32[512,1408]{1,0:T(8,128)}) async-done(((f32[512,1408]{1,0:T(8,128)}, f32[512,1408]{1,0:T(8,128)}), (f32[512,1408]{1,0:T(8,128)}, f32[512,1408]{1,0:T(8,128)})) %all-reduce.9.cloned.1.call-update) | async-done | bytes 5767184 | tf_op jit(solution)/shard_map/psum | solution.py:46
  142.6 2.3 multiply_multiply_fusion.1
  144.8 1.2 copy-done
  146.1 6.0 fusion.3
  152.3 227.4 %all-gather.5.cloned.1.call-done = f32[4096,1024]{1,0:T(8,128)} async-done(((f32[512,1024]{1,0:T(8,128)}), f32[4096,1024]{1,0:T(8,128)}) %all-gather.5.cloned.1.call-update) | async-done | bytes 16777232 | tf_op jit(solution)/shard_map/all_gather | solution.py:13
  379.7 8.0 %reduce_sum.37 = f32[512,1024]{1,0:T(8,128)S(1)} reduce(f32[8,512,1024]{2,1,0:T(8,128)} %bitcast.24, f32[]{:T(128)} %constant.12.clone.1), dimensions={0}, to_apply=%region_4.5 | reduce | flops 3670016 | bytes 18874372 | tf_op jit(solution)/shard_map/reduce_sum | solution.py:14
  387.7 1.9 fusion.13
  389.6 5.3 fusion.2
  394.9 3.5 fusion.1
  398.5 5.9 psum.46
  404.3 103.5 %all-reduce.7.cloned.1.call-done = (f32[512,1408]{1,0:T(8,128)}, f32[512,1408]{1,0:T(8,128)}) async-done(((f32[512,1408]{1,0:T(8,128)}, f32[512,1408]{1,0:T(8,128)}), (f32[512,1408]{1,0:T(8,128)}, f32[512,1408]{1,0:T(8,128)})) %all-reduce.7.cloned.1.call-update) | async-done | bytes 5767184 | tf_op jit(solution)/shard_map/psum | solution.py:46
  507.8 2.3 multiply_multiply_fusion
  510.1 0.4 copy-done.9
  510.5 6.0 fusion
  516.5 227.6 %all-gather.7.cloned.1.call-done = f32[4096,1024]{1,0:T(8,128)} async-done(((f32[512,1024]{1,0:T(8,128)}), f32[4096,1024]{1,0:T(8,128)}) %all-gather.7.cloned.1.call-update) | async-done | bytes 16777232 | tf_op jit(solution)/shard_map/all_gather | solution.py:13
  744.1 8.0 %reduce_sum.39 = f32[512,1024]{1,0:T(8,128)S(1)} reduce(f32[8,512,1024]{2,1,0:T(8,128)} %bitcast.25, f32[]{:T(128)} %constant.12.clone.1), dimensions={0}, to_apply=%region_9.10 | reduce | flops 3670016 | bytes 18874372 | tf_op jit(solution)/shard_map/reduce_sum | solution.py:14
  752.1 1.3 fusion.11
  (38 shorter events, 0.9 us)
Async XLA Ops:
  6.5 136.0 %all-reduce.9.cloned.1.call-start = ((), (), s32[]{:S(2)}) async-start(), calls=%async_computation.3 | async-start | bytes 11534336 | tf_op jit(solution)/shard_map/psum | solution.py:46
  12.2 9.4 %copy-start.1 = (bf16[2,1024,1408]{2,1,0:T(8,128)(2,1)}, bf16[2,1024,1408]{2,1,0:T(8,128)(2,1)S(1)}, u32[]{:S(2)}) copy-start(bf16[2,1024,1408]{2,1,0:T(8,128)(2,1)S(1)} %convert.13) | copy-start | bytes 17301508
  12.2 9.4 %copy-start.3 = (bf16[512,1024]{1,0:T(8,128)(2,1)S(1)}, bf16[512,1024]{1,0:T(8,128)(2,1)}, u32[]{:S(2)}) copy-start(bf16[512,1024]{1,0:T(8,128)(2,1)} %param.10) | copy-start | bytes 3145732
  21.6 3.4 copy-start.2
  28.5 17.2 %copy-start.5 = (f32[2,1408]{1,0:T(2,128)S(1)}, f32[2,1408]{1,0:T(2,128)}, u32[]{:S(2)}) copy-start(f32[2,1408]{1,0:T(2,128)} %param.14) | copy-start | bytes 33796
  28.5 17.2 %copy-start.6 = (f32[2,1408]{1,0:T(2,128)S(1)}, f32[2,1408]{1,0:T(2,128)}, u32[]{:S(2)}) copy-start(f32[2,1408]{1,0:T(2,128)} %param.15) | copy-start | bytes 33796
  28.5 17.2 %copy-start.7 = (f32[2,1408]{1,0:T(2,128)S(1)}, f32[2,1408]{1,0:T(2,128)}, u32[]{:S(2)}) copy-start(f32[2,1408]{1,0:T(2,128)} %param.19) | copy-start | bytes 33796
  28.5 17.3 %copy-start.4 = (f32[2,3,1408]{2,0,1:T(2,128)S(1)}, f32[2,3,1408]{2,0,1:T(2,128)}, u32[]{:S(2)}) copy-start(f32[2,3,1408]{2,0,1:T(2,128)} %param.18) | copy-start | bytes 101380
  28.5 351.2 %all-gather.5.cloned.1.call-start = ((), (), s32[]{:S(2)}) async-start(), calls=%async_computation | async-start | bytes 18874368 | tf_op jit(solution)/shard_map/all_gather | solution.py:13
  142.6 3.5 copy-start
  146.1 6.2 copy-start.8
  152.1 355.7 %all-reduce.7.cloned.1.call-start = ((), (), s32[]{:S(2)}) async-start(), calls=%async_computation.2 | async-start | bytes 11534336 | tf_op jit(solution)/shard_map/psum | solution.py:46
  387.7 7.2 slice-start
  389.6 5.3 slice-start.1
  398.4 345.7 %all-gather.7.cloned.1.call-start = ((), (), s32[]{:S(2)}) async-start(), calls=%async_computation.1 | async-start | bytes 18874368 | tf_op jit(solution)/shard_map/all_gather | solution.py:13
  507.8 2.7 copy-start.9
Sparse Core Ops, SparseCore 0:
  28.6 113.9 all-reduce.8
  152.2 227.4 all-gather.4
  398.5 109.2 all-reduce.6
  516.6 227.4 all-gather.6
